TPU v7x, 32 devices: a whole 2x2x4 slice. The times are simulated.
32 devices in a mesh: st: 4 (over y, x), tp: 8 (over z, core).
Axes of the slice: x: 2, y: 2, z: 4, core: 2. Of those that a mesh axis runs over, the one named last changes fastest.
Arguments:
- normed: bfloat16 [2048, 2048], P('st'), may hold values from -128 to 128
- store: bfloat16 [8192, 2048], P('st'), may hold values from -5 to 5
- passage_ids: int32 [16, 2], P('st'), may hold values from 0 to 127, as said below
- w_query: bfloat16 [2048, 2048], P(None, 'tp'), as said below
- w_gate: bfloat16 [2048, 2048], P(None, 'tp'), may hold values from -0.125 to 0.125
- w_key: bfloat16 [2048, 2048], P(None, 'tp'), as said below
- w_value: bfloat16 [2048, 2048], P(None, 'tp'), may hold values from -0.125 to 0.125
- cotangent: bfloat16 [2048, 2048], P('st', 'tp'), may hold values from -6 to 6
Outputs:
- grad_rows: float32 [2048, 2048], P('st', 'tp')
- grad_store: float32 [8192, 2048], P('st', 'tp')
- grad_query_weight: float32 [2048, 2048], P('st', 'tp')
Inputs may be any that keep to these rules, and one draw needn't show every extreme that they name: `passage_ids`: each row names 2 passages. The passages read by the blocks of one index of st are all different, and at most 4 of them belong to any one owner (the owner of passage p is the index p // 32 of st). In every draw some owner has one of its passages read by every index of st. `w_query`: entries lie within 6 * 2048 ** -0.5 in magnitude. `w_key`: entries lie within 8 * 2048 ** -0.5 in magnitude.
All inputs are finite; a program needn't handle non-finite values.
Results may differ from a plain program's by a relative error of at most 0.019.
Values may be sent and summed in bfloat16 or wider, within the bound.
A program may use at most 128 MiB of HBM per device.

v0:
```python
import functools

import jax
import jax.numpy as jnp
from jax import lax
from jax.experimental import pallas as pl
from jax.experimental.pallas import tpu as pltpu
from jax.sharding import PartitionSpec as P

DH = 128
BLK = 128
PLEN = 64
GROUP = 4
CORES = 2
F32 = jnp.float32
BF16 = jnp.bfloat16
MESH = pl.DeviceIdType.MESH


def dot_nn(a, b):
    return lax.dot_general(a, b, (((1,), (0,)), ((), ())), preferred_element_type=F32)


def dot_nt(a, b):
    return lax.dot_general(a, b, (((1,), (1,)), ((), ())), preferred_element_type=F32)


def dot_tn(a, b):
    return lax.dot_general(a, b, (((0,), (0,)), ((), ())), preferred_element_type=F32)


def rows_at(index, size):
    return pl.ds(pl.multiple_of(index * size, size), size)


def project_kernel(ids, *refs):
    passages = refs[:GROUP]
    wk_ref, wv_ref, out_ref = refs[GROUP:]
    rows = jnp.concatenate([p[...] for p in passages], axis=0)
    width = wk_ref.shape[1]
    out_ref[:, :width] = dot_nn(rows, wk_ref[...]).astype(BF16)
    out_ref[:, width:] = dot_nn(rows, wv_ref[...]).astype(BF16)


def project(store, ids, w_key, w_value):
    slots = ids.shape[0]
    depth, width = w_key.shape
    passage = lambda g: pl.BlockSpec((PLEN, depth), lambda i, ids: (ids[GROUP * i + g], 0))
    weight = pl.BlockSpec((depth, width), lambda i, ids: (0, 0))
    return pl.pallas_call(
        project_kernel,
        out_shape=jax.ShapeDtypeStruct((slots * PLEN, 2 * width), BF16),
        grid_spec=pltpu.PrefetchScalarGridSpec(
            num_scalar_prefetch=1,
            grid=(slots // GROUP,),
            in_specs=[passage(g) for g in range(GROUP)] + [weight, weight],
            out_specs=pl.BlockSpec((GROUP * PLEN, 2 * width), lambda i, ids: (i, 0)),
        ),
        compiler_params=pltpu.CompilerParams(vmem_limit_bytes=58 << 20),
        name="project",
    )(ids, *([store] * GROUP), w_key, w_value)


def main_kernel(
    st_n, tp_n, reads,
    slot_of, req_of, served, normed_h, w_q_h, w_g_h, w_k_h, w_v_h, cot_h,
    rows_out, ret_out, gqw_out,
    normed, w_q, w_g, w_k, w_v, cot, load_sem,
    arrived, q_s, gate_s, dq_s, dg_s, dp_s,
    x_out, x_in, z_out, up_in, dn_in, own, part, r_out, r_in, g_out, g_in, g_own,
    kv_ss, kv_rs, x_ss, x_rs, z_ss, up_rs, dn_rs, r_ss, r_rs, g_ss, g_rs,
):
    me_st, me_tp = lax.axis_index("st"), lax.axis_index("tp")
    z_n = tp_n // CORES
    me_z, me_c = me_tp // CORES, me_tp % CORES
    mate = (me_st, me_z * CORES + 1 - me_c)
    tok, hw = cot.shape
    depth = w_q.shape[0]
    heads = hw // DH
    blocks = tok // BLK
    cw = depth // tp_n
    slots = served.shape[0] // st_n
    scale = DH ** (-0.5)

    def st_peer(d):
        return lax.rem(me_st + d, st_n)

    def st_from(d):
        return lax.rem(me_st + st_n - d, st_n)

    def z_peer(d):
        return lax.rem(me_z + d, z_n)

    loads = []
    pairs = ((normed_h, normed), (w_q_h, w_q), (w_g_h, w_g), (cot_h, cot), (w_k_h, w_k), (w_v_h, w_v))
    for i, (far, near) in enumerate(pairs):
        loads.append(pltpu.make_async_copy(far, near, load_sem.at[i]))
        loads[-1].start()

    barrier = pltpu.get_barrier_semaphore()
    for d in range(1, st_n):
        pl.semaphore_signal(barrier, inc=1, device_id=(st_peer(d), me_tp), device_id_type=MESH)
    for d in range(1, z_n):
        pl.semaphore_signal(
            barrier, inc=1, device_id=(me_st, z_peer(d) * CORES + me_c), device_id_type=MESH
        )
    pl.semaphore_signal(barrier, inc=1, device_id=mate, device_id_type=MESH)
    pl.semaphore_wait(barrier, st_n + z_n - 1)

    def remote(src, dst, ss, rs, dev):
        return pltpu.make_async_remote_copy(
            src_ref=src, dst_ref=dst, send_sem=ss, recv_sem=rs, device_id=dev, device_id_type=MESH
        )

    sends = []

    def go(copy):
        copy.start()
        sends.append(copy)

    for d in range(1, st_n):
        go(remote(
            served.at[rows_at(st_peer(d), slots)], arrived.at[rows_at(me_st, slots)],
            kv_ss.at[d], kv_rs.at[d], (st_peer(d), me_tp),
        ))
    arrived[rows_at(me_st, slots)] = served[rows_at(me_st, slots)]

    for load in loads:
        load.wait()
    tile = 2 * BLK

    @pl.loop(0, tok // tile)
    def _(i):
        span = rows_at(i, tile)
        q_s[span, :] = dot_nn(normed[span, :], w_q[...]).astype(BF16)
        gate_s[span, :] = jax.nn.sigmoid(dot_nn(normed[span, :], w_g[...]))

    for d in range(1, st_n):
        here = arrived.at[rows_at(st_from(d), slots)]
        remote(here, here, kv_ss.at[d], kv_rs.at[d], (st_peer(d), me_tp)).wait_recv()

    for b in range(blocks):
        kv = jnp.concatenate(
            [arrived[slot_of[b * reads + r]] for r in range(reads)], axis=0
        )
        toks = slice(b * BLK, (b + 1) * BLK)
        span = reads * PLEN
        ctx = slice(b * span, (b + 1) * span)
        for h in range(heads):
            ch = slice(h * DH, (h + 1) * DH)
            chv = slice(hw + h * DH, hw + (h + 1) * DH)
            k, v = kv[:, ch], kv[:, chv]
            q = q_s[toks, ch]
            gate = gate_s[toks, ch]
            up = cot[toks, ch].astype(F32)
            s = dot_nt(q, k) * scale
            e = jnp.exp(s - jnp.max(s, axis=1, keepdims=True))
            p = e / jnp.sum(e, axis=1, keepdims=True)
            low = p.astype(BF16)
            att = dot_nn(low, v)
            d_att = (up * gate).astype(BF16)
            dg_s[toks, ch] = (up * att * gate * (1.0 - gate)).astype(BF16)
            dp_s[ctx, chv] = dot_tn(low, d_att).astype(BF16)
            d_p = dot_nt(d_att, v)
            delta = jnp.sum(d_p * p, axis=1, keepdims=True)
            d_s = (p * (d_p - delta) * scale).astype(BF16)
            dq_s[toks, ch] = dot_nn(d_s, k).astype(BF16)
            dp_s[ctx, ch] = dot_tn(d_s, q).astype(BF16)

    def chunk(which, t):
        w_rows = rows_at(t, cw)
        if which == 0:
            return dot_nt(dp_s[:, :hw], w_k[w_rows, :]) + dot_nt(dp_s[:, hw:], w_v[w_rows, :])
        return dot_nt(dq_s[...], w_q[w_rows, :]) + dot_nt(dg_s[...], w_g[w_rows, :])

    order = []
    for i in range((z_n + 1) // 2):
        order += [z_n - 1 - i, i] if z_n - 1 - i != i else [i]
    above, below = me_z < z_n - 1, me_z > 0

    def mate_stage(which, t):
        n = which * z_n + t
        x_out[n] = chunk(which, t * CORES + 1 - me_c).astype(BF16)
        go(remote(x_out.at[n], x_in.at[n], x_ss.at[n], x_rs.at[n], mate))

    def hop(n, up):
        landing, rs = (up_in, up_rs) if up else (dn_in, dn_rs)
        to = me_z + 1 if up else me_z - 1
        return remote(
            z_out.at[n], landing.at[n], z_ss.at[n], rs.at[n], (me_st, to * CORES + me_c)
        )

    def chip_stage(which, t):
        if True:
            n = which * z_n + t
            mine = chunk(which, t * CORES + me_c)
            remote(x_in.at[n], x_in.at[n], x_ss.at[n], x_rs.at[n], mate).wait_recv()
            total = mine + x_in[n].astype(F32)
            own[n] = total

            @pl.when(jnp.logical_and(me_z == 0, t > me_z))
            def _():
                z_out[n] = total.astype(BF16)
                hop(n, True).start()

            @pl.when(jnp.logical_and(me_z == z_n - 1, t < me_z))
            def _():
                z_out[n] = total.astype(BF16)
                hop(n, False).start()

    def relay_stage(which):
        for t in order:
            n = which * z_n + t

            @pl.when(jnp.logical_and(below, t > me_z))
            def _():
                hop(n, True).wait_recv()
                z_out[n] = (own[n] + up_in[n].astype(F32)).astype(BF16)
                hop(n, True).start()

            @pl.when(jnp.logical_and(above, t < me_z))
            def _():
                hop(n, False).wait_recv()
                z_out[n] = (own[n] + dn_in[n].astype(F32)).astype(BF16)
                hop(n, False).start()

    def gathered(which, put):
        for t in range(z_n):
            n = which * z_n + t

            @pl.when(t == me_z)
            def _():
                if t > 0:
                    hop(n, True).wait_recv()
                if t < z_n - 1:
                    hop(n, False).wait_recv()
                total = own[n]
                if t > 0:
                    total = total + up_in[n].astype(F32)
                if t < z_n - 1:
                    total = total + dn_in[n].astype(F32)
                put(total)

    def put_part(total):
        part[...] = total.astype(BF16).reshape(part.shape)

    def put_rows(total):
        rows_out[...] = total

    ahead = 2
    queue = [(which, t) for which in range(2) for t in order]
    for i in range(len(queue) + ahead):
        if i < len(queue):
            mate_stage(*queue[i])
        if i >= ahead:
            chip_stage(*queue[i - ahead])

    relay_stage(0)
    dw = depth // st_n
    for d in list(range(1, st_n)) + [0]:
        term = dot_tn(normed[:, rows_at(st_peer(d), dw)], dq_s[...])
        if d == 0:
            g_own[...] = term
        else:
            g_out[d] = term.astype(BF16)
            go(remote(
                g_out.at[d], g_in.at[d], g_ss.at[d], g_rs.at[d], (st_peer(d), me_tp)
            ))

    gathered(0, put_part)
    for s in range(st_n * slots):
        r_out[s] = part[req_of[s]]
    for d in range(1, st_n):
        go(remote(
            r_out.at[rows_at(st_peer(d), slots)], r_in.at[rows_at(me_st, slots)],
            r_ss.at[d], r_rs.at[d], (st_peer(d), me_tp),
        ))
    ret_out[rows_at(me_st, slots)] = r_out[rows_at(me_st, slots)]

    relay_stage(1)
    total = g_own[...]
    for d in range(1, st_n):
        remote(g_in.at[d], g_in.at[d], g_ss.at[d], g_rs.at[d], (st_peer(d), me_tp)).wait_recv()
        total = total + g_in[d].astype(F32)
    gqw_out[...] = total

    for d in range(1, st_n):
        span = rows_at(st_from(d), slots)
        remote(
            r_in.at[span], r_in.at[span], r_ss.at[d], r_rs.at[d], (st_peer(d), me_tp)
        ).wait_recv()
        ret_out[span] = r_in[span]

    gathered(1, put_rows)
    for copy in sends:
        copy.wait_send()
    for t in range(z_n):
        for which in range(2):

            @pl.when(t != me_z)
            def _():
                hop(which * z_n + t, True).wait_send()


def main_call(st_n, tp_n, reads, slot_of, req_of, served, normed, w_q, w_g, w_k, w_v, cot):
    tok, hw = cot.shape
    depth = w_q.shape[0]
    cw, dw, z_n = depth // tp_n, depth // st_n, tp_n // CORES
    ctx = tok // BLK * reads * PLEN
    slot_total = served.shape[0]
    vmem = pl.BlockSpec(memory_space=pltpu.VMEM)
    smem = pl.BlockSpec(memory_space=pltpu.SMEM)
    piece = lambda rows, n=2 * z_n: pltpu.VMEM((n, rows, cw), BF16)
    sem = lambda n: pltpu.SemaphoreType.DMA((n,))
    rows_most = max(ctx, tok)
    assert ctx == tok
    return pl.pallas_call(
        functools.partial(main_kernel, st_n, tp_n, reads),
        out_shape=(
            jax.ShapeDtypeStruct((tok, cw), F32),
            jax.ShapeDtypeStruct((slot_total, PLEN, cw), BF16),
            jax.ShapeDtypeStruct((dw, hw), F32),
        ),
        in_specs=[smem, smem, vmem] + [pl.BlockSpec(memory_space=pl.ANY)] * 6,
        out_specs=(vmem, vmem, vmem),
        scratch_shapes=[
            *[pltpu.VMEM(a.shape, a.dtype) for a in (normed, w_q, w_g, w_k, w_v, cot)],
            sem(6),
            pltpu.VMEM((slot_total, PLEN, 2 * hw), BF16),
            pltpu.VMEM((tok, hw), BF16),
            pltpu.VMEM((tok, hw), F32),
            pltpu.VMEM((tok, hw), BF16),
            pltpu.VMEM((tok, hw), BF16),
            pltpu.VMEM((ctx, 2 * hw), BF16),
            piece(rows_most), piece(rows_most), piece(rows_most), piece(rows_most), piece(rows_most),
            pltpu.VMEM((2 * z_n, rows_most, cw), F32),
            pltpu.VMEM((ctx // PLEN, PLEN, cw), BF16),
            pltpu.VMEM((slot_total, PLEN, cw), BF16),
            pltpu.VMEM((slot_total, PLEN, cw), BF16),
            pltpu.VMEM((st_n, dw, hw), BF16),
            pltpu.VMEM((st_n, dw, hw), BF16),
            pltpu.VMEM((dw, hw), F32),
            sem(st_n), sem(st_n), sem(2 * z_n), sem(2 * z_n), sem(2 * z_n), sem(2 * z_n), sem(2 * z_n),
            sem(st_n), sem(st_n), sem(st_n), sem(st_n),
        ],
        compiler_params=pltpu.CompilerParams(
            collective_id=0, has_side_effects=True, vmem_limit_bytes=56 << 20
        ),
        name="main",
    )(slot_of, req_of, served, normed, w_q, w_g, w_k, w_v, cot)


def spread_kernel(ids, returned, rows, gqw, out_ref, rows_ref, gqw_ref):
    rows_ref[...] = rows[...]
    gqw_ref[...] = gqw[...]
    out_ref[...] = jnp.zeros_like(out_ref)
    for s in range(ids.shape[0]):
        passage = ids[s]

        @pl.when(passage >= 0)
        def _():
            span = rows_at(passage, PLEN)
            out_ref[span, :] += returned[s].astype(F32)


def spread(ids, returned, grad_rows, grad_query_weight, rows):
    vmem = pl.BlockSpec(memory_space=pltpu.VMEM)
    return pl.pallas_call(
        spread_kernel,
        out_shape=(
            jax.ShapeDtypeStruct((rows, returned.shape[2]), F32),
            jax.ShapeDtypeStruct(grad_rows.shape, F32),
            jax.ShapeDtypeStruct(grad_query_weight.shape, F32),
        ),
        in_specs=[pl.BlockSpec(memory_space=pltpu.SMEM), vmem, vmem, vmem],
        out_specs=(vmem, vmem, vmem),
        compiler_params=pltpu.CompilerParams(vmem_limit_bytes=60 << 20),
        name="spread",
    )(ids, returned, grad_rows, grad_query_weight)


def shards(normed, store, passage_ids, w_query, w_gate, w_key, w_value, cotangent):
    peer_count = lax.axis_size("st")
    blocks, read_count = passage_ids.shape
    requests = blocks * read_count
    slot_most = max(1, 2 * requests // peer_count)
    slot_count = peer_count * slot_most
    pass_dev = store.shape[0] // PLEN
    flat_ids = passage_ids.reshape(requests)
    owners = flat_ids // pass_dev
    local_ids = flat_ids % pass_dev
    positions = jnp.arange(requests, dtype=jnp.int32)
    before = (owners[:, None] == owners[None, :]) & (positions[None, :] < positions[:, None])
    slot_of = owners * slot_most + jnp.sum(before.astype(jnp.int32), axis=1)
    slot_hit = slot_of[:, None] == jnp.arange(slot_count, dtype=jnp.int32)[None, :]
    slot_table = jnp.max(jnp.where(slot_hit, local_ids[:, None], -1), axis=0)
    req_of = jnp.max(jnp.where(slot_hit, positions[:, None], 0), axis=0)
    served_ids = lax.all_to_all(
        slot_table.reshape(peer_count, slot_most), "st", split_axis=0, concat_axis=0, tiled=True
    ).reshape(slot_count)
    served = project(store, jnp.maximum(served_ids, 0), w_key, w_value)
    served = served.reshape(slot_count, PLEN, served.shape[1])
    grad_rows, returned, grad_query_weight = main_call(
        peer_count, lax.axis_size("tp"), read_count,
        slot_of, req_of, served, normed, w_query, w_gate, w_key, w_value, cotangent,
    )
    grad_store, grad_rows, grad_query_weight = spread(
        served_ids, returned, grad_rows, grad_query_weight, store.shape[0]
    )
    return (grad_rows, grad_store, grad_query_weight)


def solution(mesh):
    placed = (
        P("st", None),
        P("st", None),
        P("st", None),
        P(None, "tp"),
        P(None, "tp"),
        P(None, "tp"),
        P(None, "tp"),
        P("st", "tp"),
    )
    return jax.shard_map(
        shards,
        mesh=mesh,
        in_specs=placed,
        out_specs=(P("st", "tp"), P("st", "tp"), P("st", "tp")),
        check_vma=False,
    )
```

profile of v0, /device:TPU:0, one launch (start us, length us, event | category | flops | bytes accessed | tf_op | source)
XLA Modules:
  0.0 89.7 jit_solution(8912154452933160344)
XLA Ops:
  0.6 0.8 copy.15
  1.4 0.1 reshape.110
  1.5 0.2 convert_reduce_fusion
  1.7 0.0 copy-start.1
  1.7 0.6 select_reduce_fusion
  2.3 0.1 all_to_all.6
  2.4 9.7 %all_to_all.9 = s32[4,1,4]{2,1,0:T(1,128)S(1)} all-to-all(s32[4,1,4]{2,1,0:T(1,128)S(1)} %bitcast.3), channel_id=1, replica_groups=mesh['st'=4,'tp'=8] {'st'}, dimensions={0} | all-to-all | bytes 128 | tf_op jit(solution)/shard_map/all_to_all | solution.py:398
  12.0 0.5 broadcast.133
  12.5 0.7 reduce.3
  13.2 0.1 reshape.111.ids
  13.3 0.0 copy-start
  13.3 0.5 broadcast_maximum_fusion.ids
  13.8 6.8 %project.1 = bf16[1024,512]{1,0:T(8,128)(2,1)} custom-call(s32[16]{0:T(128)} %broadcast_maximum_fusion.ids, bf16[2048,2048]{1,0:T(8,128)(2,1)} %refs_3_.1, bf16[2048,2048]{1,0:T(8,128)(2,1)} %refs_3_.1, bf16[2048,2048]{1,0:T(8,128)(2,1)} %refs_3_.1, bf16[2048,2048]{1,0:T(8,128)(2,1)} %refs_3_.1, bf16[2048,256]{1,0:T(8,128)(2,1)} %w_k_h.1, ...), custom_call_target="tpu_custom_call" | custom-call | tf_op jit(solution)/shard_map/project/pallas_call | solution.py:50
  20.6 0.0 copy-done.1
  20.6 0.0 copy-done
  20.6 65.8 %main.1 = (f32[512,256]{1,0:T(8,128)}, bf16[16,64,256]{2,1,0:T(8,128)(2,1)}, f32[512,256]{1,0:T(8,128)}) custom-call(s32[8]{0:T(128)} %copy-done.1, s32[16]{0:T(128)} %get-tuple-element.15.req_of, bf16[16,64,512]{2,1,0:T(8,128)(2,1)} %bitcast.2, bf16[512,2048]{1,0:T(8,128)(2,1)} %normed_h.1, bf16[2048,256]{1,0:T(8,128)(2,1)} %w_q_h.1, ...), custom_call_target="tpu_custom_call" | custom-call | tf_op jit(solution)/shard_map/main/pallas_call | solution.py:317
  86.4 3.4 %spread.1 = (f32[2048,256]{1,0:T(8,128)}, f32[512,256]{1,0:T(8,128)}, f32[512,256]{1,0:T(8,128)}) custom-call(s32[16]{0:T(128)} %copy-done, bf16[16,64,256]{2,1,0:T(8,128)(2,1)} %get-tuple-element.9.returned, f32[512,256]{1,0:T(8,128)} %get-tuple-element.10.rows, f32[512,256]{1,0:T(8,128)} %get-tuple-element.11.gqw), custom_call_target="tpu_custom_call" | custom-call | tf_op jit(solution)/shard_map/spread/pallas_call | solution.py:368
  (2 shorter events, 0.0 us)
Async XLA Ops:
  1.7 18.9 %copy-start.1 = (s32[8]{0:T(128)}, s32[8]{0:T(128)S(1)}, u32[]{:S(2)}) copy-start(s32[8]{0:T(128)S(1)} %multiply_add_fusion.slot_of) | copy-start | bytes 100
  13.3 7.3 %copy-start = (s32[16]{0:T(128)}, s32[16]{0:T(128)S(1)}, u32[]{:S(2)}) copy-start(s32[16]{0:T(128)S(1)} %reshape.111.ids) | copy-start | bytes 196
where the time goes:
time: 90 us; the launch traced here: 89.7 us
  Pallas kernels  75.9 us (84%)
  blocking collectives  9.66 us (11%)
  other arithmetic  1.98 us (2%)
  local copies, waits for them, and re-layouts  1.54 us (2%)
    pallas_call x1, Pallas kernels, main_call(): pl.pallas_call(functools.partial(main_kernel, st_n, tp_n, reads), out_sha...  65.8 us
    all_to_all x1, blocking collectives, shards(): lax.all_to_all(slot_table.reshape(peer_count, slot_most), 'st', split_axi...  9.66 us
    pallas_call x1, Pallas kernels, project(): pl.pallas_call(project_kernel, out_shape=jax.ShapeDtypeStruct((slots * PL...  6.76 us
    pallas_call x1, Pallas kernels, spread(): pl.pallas_call(spread_kernel, out_shape=(jax.ShapeDtypeStruct((rows, retu...  3.37 us

commit v1 on v0

v1 whole, which is shorter than its diff:
```python
import functools

import jax
import jax.numpy as jnp
from jax import lax
from jax.experimental import pallas as pl
from jax.experimental.pallas import tpu as pltpu
from jax.sharding import PartitionSpec as P

DH = 128
BLK = 128
PLEN = 64
GROUP = 4
CORES = 2
F32 = jnp.float32
BF16 = jnp.bfloat16
MESH = pl.DeviceIdType.MESH


def dot_nn(a, b):
    return lax.dot_general(a, b, (((1,), (0,)), ((), ())), preferred_element_type=F32)


def dot_nt(a, b):
    return lax.dot_general(a, b, (((1,), (1,)), ((), ())), preferred_element_type=F32)


def dot_tn(a, b):
    return lax.dot_general(a, b, (((0,), (0,)), ((), ())), preferred_element_type=F32)


def rows_at(index, size):
    return pl.ds(pl.multiple_of(index * size, size), size)


def main_kernel(
    st_n, tp_n, reads, slots, pass_dev,
    ids, store_h, normed_h, w_q_h, w_g_h, w_k_h, w_v_h, cot_h,
    rows_out, ret_out, gqw_out, served_out,
    store, normed, w_q, w_g, w_k, w_v, cot, load_sem,
    mine, tables, req_of, slot_of, early_of, t_ss, t_rs,
    served, arr_e, arr_all, q_s, gate_s, dq_s, dg_s, dp_s,
    x_out, x_in, z_out, up_in, dn_in, own, part, r_out, r_in, g_out, g_in, g_own,
    kv_ss, kv_rs, x_ss, x_rs, z_ss, up_rs, dn_rs, r_ss, r_rs, g_ss, g_rs,
):
    me_st, me_tp = lax.axis_index("st"), lax.axis_index("tp")
    z_n = tp_n // CORES
    me_z, me_c = me_tp // CORES, me_tp % CORES
    mate = (me_st, me_z * CORES + 1 - me_c)
    tok, hw = cot.shape
    depth = w_q.shape[0]
    heads = hw // DH
    blocks = tok // BLK
    cw = depth // tp_n
    first = min(reads, slots)
    n_pos = blocks * reads
    scale = DH ** (-0.5)

    def st_peer(d):
        return lax.rem(me_st + d, st_n)

    def st_from(d):
        return lax.rem(me_st + st_n - d, st_n)

    def load(i, far, near):
        copy = pltpu.make_async_copy(far, near, load_sem.at[i])
        copy.start()
        return copy

    loads_a = [
        load(i, far, near)
        for i, (far, near) in enumerate(((w_k_h, w_k), (store_h, store), (w_v_h, w_v)))
    ]

    above, below = me_z < z_n - 1, me_z > 0
    barrier = pltpu.get_barrier_semaphore()

    def greet(device):
        pl.semaphore_signal(barrier, inc=1, device_id=device, device_id_type=MESH)

    for d in range(1, st_n):
        greet((st_peer(d), me_tp))

    @pl.when(above)
    def _():
        greet((me_st, (me_z + 1) * CORES + me_c))

    @pl.when(below)
    def _():
        greet((me_st, (me_z - 1) * CORES + me_c))

    greet(mate)

    passages = [ids[i % reads, i // reads] for i in range(n_pos)]
    owners = [lax.div(p, jnp.int32(pass_dev)) for p in passages]
    ranks = []
    for i in range(n_pos):
        rank = jnp.int32(0)
        for j in range(i):
            rank = rank + jnp.where(owners[j] == owners[i], 1, 0)
        ranks.append(rank)
    places = [owners[i] * slots + ranks[i] for i in range(n_pos)]
    for i in range(n_pos):
        slot_of[i] = places[i]
        early_of[i] = owners[i] * first + jnp.minimum(ranks[i], first - 1)
    for s in range(st_n * slots):
        local, position = jnp.int32(-1), jnp.int32(0)
        for i in range(n_pos):
            hit = places[i] == s
            local = jnp.where(hit, passages[i] - (s // slots) * pass_dev, local)
            position = jnp.where(hit, i, position)
        mine[s] = local
        req_of[s] = position

    pl.semaphore_wait(
        barrier, st_n + jnp.where(above, 1, 0) + jnp.where(below, 1, 0)
    )

    def remote(src, dst, ss, rs, dev):
        return pltpu.make_async_remote_copy(
            src_ref=src, dst_ref=dst, send_sem=ss, recv_sem=rs, device_id=dev, device_id_type=MESH
        )

    sends = []

    def go(copy):
        copy.start()
        sends.append(copy)

    for d in range(1, st_n):
        go(remote(mine, tables.at[d], t_ss.at[d], t_rs.at[d], (st_peer(d), me_tp)))
    loads_b = [
        load(3 + i, far, near)
        for i, (far, near) in enumerate(
            ((normed_h, normed), (w_q_h, w_q), (w_g_h, w_g), (cot_h, cot))
        )
    ]
    for copy in loads_a:
        copy.wait()
    for d in range(1, st_n):
        remote(tables.at[d], tables.at[d], t_ss.at[d], t_rs.at[d], (st_peer(d), me_tp)).wait_recv()

    def wanted(d, k):
        at = me_st * slots + k
        return tables[st_n - d, at] if d else mine[at]

    dists = list(range(1, st_n)) + [0]

    def kv_copy(d, k, outgoing):
        owner = me_st if outgoing else st_from(d)
        landing = arr_e.at[owner * first + k] if k < first else arr_all.at[owner * slots + k]
        n = d * slots + k
        source = served.at[n] if outgoing else landing
        return remote(source, landing, kv_ss.at[n], kv_rs.at[n], (st_peer(d), me_tp))

    def project(k, some):
        rows = jnp.concatenate(
            [store[jnp.maximum(wanted(d, k), 0)] for d in some], axis=0
        )
        keys = dot_nn(rows, w_k[...]).astype(BF16)
        values = dot_nn(rows, w_v[...]).astype(BF16)
        for i, d in enumerate(some):
            span = slice(i * PLEN, (i + 1) * PLEN)
            if d:
                served[d * slots + k, :, :hw] = keys[span]
                served[d * slots + k, :, hw:] = values[span]
                go(kv_copy(d, k, True))
            elif k < first:
                arr_e[me_st * first + k, :, :hw] = keys[span]
                arr_e[me_st * first + k, :, hw:] = values[span]
            else:
                arr_all[me_st * slots + k, :, :hw] = keys[span]
                arr_all[me_st * slots + k, :, hw:] = values[span]

    for k in range(slots):
        for i in range(0, st_n, GROUP):
            project(k, dists[i:i + GROUP])

    for d in range(st_n):
        for k in range(slots):
            served_out[st_peer(d) * slots + k] = wanted(d, k)

    for copy in loads_b:
        copy.wait()
    tile = 2 * BLK

    @pl.loop(0, tok // tile)
    def _(i):
        span = rows_at(i, tile)
        q_s[span, :] = dot_nn(normed[span, :], w_q[...]).astype(BF16)
        gate_s[span, :] = jax.nn.sigmoid(dot_nn(normed[span, :], w_g[...]))

    def kv_arrived(ranks):
        for k in ranks:
            for d in range(1, st_n):
                kv_copy(d, k, False).wait_recv()

    span = reads * PLEN

    def attend(b):
        if b == 0 or slots == first:
            parts = [arr_e[early_of[b * reads + r]] for r in range(reads)]
        else:
            parts = [arr_all[slot_of[b * reads + r]] for r in range(reads)]
        kv = jnp.concatenate(parts, axis=0)
        toks = slice(b * BLK, (b + 1) * BLK)
        ctx = slice(b * span, (b + 1) * span)
        for h in range(heads):
            ch = slice(h * DH, (h + 1) * DH)
            chv = slice(hw + h * DH, hw + (h + 1) * DH)
            k, v = kv[:, ch], kv[:, chv]
            q = q_s[toks, ch]
            gate = gate_s[toks, ch]
            up = cot[toks, ch].astype(F32)
            d_att = (up * gate).astype(BF16)
            d_p = dot_nt(d_att, v)
            s = dot_nt(q, k) * scale
            e = jnp.exp(s - jnp.max(s, axis=1, keepdims=True))
            p = e / jnp.sum(e, axis=1, keepdims=True)
            low = p.astype(BF16)
            att = dot_nn(low, v)
            dg_s[toks, ch] = (up * att * gate * (1.0 - gate)).astype(BF16)
            dp_s[ctx, chv] = dot_tn(low, d_att).astype(BF16)
            delta = jnp.sum(d_p * p, axis=1, keepdims=True)
            d_s = (p * (d_p - delta) * scale).astype(BF16)
            dq_s[toks, ch] = dot_nn(d_s, k).astype(BF16)
            dp_s[ctx, ch] = dot_tn(d_s, q).astype(BF16)

    def chunk(g, t):
        which, b = g
        w_rows = rows_at(t, cw)
        if which == 0:
            ctx = slice(b * span, (b + 1) * span)
            return dot_nt(dp_s[ctx, :hw], w_k[w_rows, :]) + dot_nt(dp_s[ctx, hw:], w_v[w_rows, :])
        toks = slice(b * BLK, (b + 1) * BLK)
        return dot_nt(dq_s[toks, :], w_q[w_rows, :]) + dot_nt(dg_s[toks, :], w_g[w_rows, :])

    order = []
    for i in range((z_n + 1) // 2):
        order += [z_n - 1 - i, i] if z_n - 1 - i != i else [i]

    def piece_of(g, t):
        return (g[0] * blocks + g[1]) * z_n + t

    def mate_copy(n):
        return remote(x_out.at[n], x_in.at[n], x_ss.at[n], x_rs.at[n], mate)

    def hop(n, up):
        landing, rs = (up_in, up_rs) if up else (dn_in, dn_rs)
        to = me_z + 1 if up else me_z - 1
        return remote(
            z_out.at[n], landing.at[n], z_ss.at[n], rs.at[n], (me_st, to * CORES + me_c)
        )

    def give(g):
        for t in order:
            n = piece_of(g, t)
            x_out[n] = chunk(g, t * CORES + 1 - me_c).astype(BF16)
            go(mate_copy(n))

    def take(g):
        for t in order:
            n = piece_of(g, t)
            own[n] = chunk(g, t * CORES + me_c)
        for t in order:
            n = piece_of(g, t)
            mate_copy(n).wait_recv()
            total = own[n] + x_in[n].astype(F32)
            own[n] = total

            @pl.when(jnp.logical_and(me_z == 0, t > me_z))
            def _():
                z_out[n] = total.astype(BF16)
                hop(n, True).start()

            @pl.when(jnp.logical_and(me_z == z_n - 1, t < me_z))
            def _():
                z_out[n] = total.astype(BF16)
                hop(n, False).start()

    def relay(g, k):
        @pl.when(me_z == k)
        def _():
            for t in range(z_n - 1, k, -1):
                n = piece_of(g, t)
                hop(n, True).wait_recv()
                z_out[n] = (own[n] + up_in[n].astype(F32)).astype(BF16)
                hop(n, True).start()

        @pl.when(me_z == z_n - 1 - k)
        def _():
            for t in range(z_n - 1 - k):
                n = piece_of(g, t)
                hop(n, False).wait_recv()
                z_out[n] = (own[n] + dn_in[n].astype(F32)).astype(BF16)
                hop(n, False).start()

    def gathered(g):
        n = piece_of(g, me_z)

        @pl.when(below)
        def _():
            hop(n, True).wait_recv()
            own[n] = own[n] + up_in[n].astype(F32)

        @pl.when(above)
        def _():
            hop(n, False).wait_recv()
            own[n] = own[n] + dn_in[n].astype(F32)

        which, b = g
        if which == 0:
            part[b * reads:(b + 1) * reads] = own[n].astype(BF16).reshape(reads, PLEN, cw)
        else:
            rows_out[b * BLK:(b + 1) * BLK, :] = own[n]

    kv_arrived(range(first))
    attend(0)
    groups = [(0, 0), (1, 0)] + [(0, b) for b in range(1, blocks)] + [(1, b) for b in range(1, blocks)]
    give(groups[0])
    give(groups[1])
    take(groups[0])
    take(groups[1])
    if slots > first:
        for o in range(st_n):
            for k in range(first):
                arr_all[o * slots + k] = arr_e[o * first + k]
        kv_arrived(range(first, slots))

    steps = len(groups) + max(z_n - 2, 0)
    relayed = [0]

    def relay_step():
        j = relayed[0]
        relayed[0] += 1
        for k in range(1, z_n - 1):
            if 0 <= j - (k - 1) < len(groups):
                relay(groups[j - (k - 1)], k)

    for b in range(1, blocks):
        attend(b)
        give((0, b))
        if b > 1:
            take((0, b - 1))
        if b == 2:
            relay_step()
    for b in range(1, blocks):
        give((1, b))
        if b == 1:
            take((0, blocks - 1))
            relay_step()
        else:
            take((1, b - 1))
    take((1, blocks - 1))
    relay_step()

    dw = depth // st_n
    for d in list(range(1, st_n)) + [0]:
        term = dot_tn(normed[:, rows_at(st_peer(d), dw)], dq_s[...])
        if d == 0:
            g_own[...] = term
        else:
            g_out[d] = term.astype(BF16)
            go(remote(
                g_out.at[d], g_in.at[d], g_ss.at[d], g_rs.at[d], (st_peer(d), me_tp)
            ))

    reads_done = max(i for i, g in enumerate(groups) if g[0] == 0) + max(z_n - 2, 1)
    while relayed[0] < min(reads_done, steps):
        relay_step()
    for b in range(blocks):
        gathered((0, b))
    for s in range(st_n * slots):
        r_out[s] = part[req_of[s]]
    for d in range(1, st_n):
        go(remote(
            r_out.at[rows_at(st_peer(d), slots)], r_in.at[rows_at(me_st, slots)],
            r_ss.at[d], r_rs.at[d], (st_peer(d), me_tp),
        ))
    ret_out[rows_at(me_st, slots)] = r_out[rows_at(me_st, slots)]

    while relayed[0] < steps - 1:
        relay_step()

    total = g_own[...]
    for d in range(1, st_n):
        remote(g_in.at[d], g_in.at[d], g_ss.at[d], g_rs.at[d], (st_peer(d), me_tp)).wait_recv()
        total = total + g_in[d].astype(F32)
    gqw_out[...] = total
    while relayed[0] < steps:
        relay_step()

    for d in range(1, st_n):
        here = rows_at(st_from(d), slots)
        remote(
            r_in.at[here], r_in.at[here], r_ss.at[d], r_rs.at[d], (st_peer(d), me_tp)
        ).wait_recv()
        ret_out[here] = r_in[here]

    for b in range(blocks):
        gathered((1, b))
    for copy in sends:
        copy.wait_send()
    for g in groups:
        for t in range(z_n):

            @pl.when(t != me_z)
            def _():
                hop(piece_of(g, t), True).wait_send()


def main_call(st_n, tp_n, ids, store, normed, w_q, w_g, w_k, w_v, cot):
    reads, blocks = ids.shape
    tok, hw = cot.shape
    depth = w_q.shape[0]
    cw, dw, z_n = depth // tp_n, depth // st_n, tp_n // CORES
    pass_dev = store.shape[0]
    n_pos = blocks * reads
    slots = max(1, 2 * n_pos // st_n)
    first = min(reads, slots)
    ctx = blocks * reads * PLEN
    slot_total = st_n * slots
    vmem = pl.BlockSpec(memory_space=pltpu.VMEM)
    smem = pl.BlockSpec(memory_space=pltpu.SMEM)
    pieces = 2 * blocks * z_n
    piece = lambda kind=BF16: pltpu.VMEM((pieces, BLK, cw), kind)
    sem = lambda n: pltpu.SemaphoreType.DMA((n,))
    table = lambda *n: pltpu.SMEM(n, jnp.int32)
    assert ctx == tok
    return pl.pallas_call(
        functools.partial(main_kernel, st_n, tp_n, reads, slots, pass_dev),
        out_shape=(
            jax.ShapeDtypeStruct((tok, cw), F32),
            jax.ShapeDtypeStruct((slot_total, PLEN, cw), BF16),
            jax.ShapeDtypeStruct((dw, hw), F32),
            jax.ShapeDtypeStruct((slot_total,), jnp.int32),
        ),
        in_specs=[smem] + [pl.BlockSpec(memory_space=pl.ANY)] * 7,
        out_specs=(vmem, vmem, vmem, smem),
        scratch_shapes=[
            *[pltpu.VMEM(a.shape, a.dtype) for a in (store, normed, w_q, w_g, w_k, w_v, cot)],
            sem(7),
            table(slot_total), table(st_n, slot_total), table(slot_total), table(n_pos), table(n_pos),
            sem(st_n), sem(st_n),
            pltpu.VMEM((slot_total, PLEN, 2 * hw), BF16),
            pltpu.VMEM((st_n * first, PLEN, 2 * hw), BF16),
            pltpu.VMEM((slot_total, PLEN, 2 * hw), BF16),
            pltpu.VMEM((tok, hw), BF16),
            pltpu.VMEM((tok, hw), F32),
            pltpu.VMEM((tok, hw), BF16),
            pltpu.VMEM((tok, hw), BF16),
            pltpu.VMEM((ctx, 2 * hw), BF16),
            piece(), piece(), piece(), piece(), piece(), piece(F32),
            pltpu.VMEM((ctx // PLEN, PLEN, cw), BF16),
            pltpu.VMEM((slot_total, PLEN, cw), BF16),
            pltpu.VMEM((slot_total, PLEN, cw), BF16),
            pltpu.VMEM((st_n, dw, hw), BF16),
            pltpu.VMEM((st_n, dw, hw), BF16),
            pltpu.VMEM((dw, hw), F32),
            sem(slot_total), sem(slot_total),
            sem(pieces), sem(pieces), sem(pieces), sem(pieces), sem(pieces),
            sem(st_n), sem(st_n), sem(st_n), sem(st_n),
        ],
        compiler_params=pltpu.CompilerParams(
            collective_id=0, has_side_effects=True, vmem_limit_bytes=56 << 20
        ),
        name="main",
    )(ids, store, normed, w_q, w_g, w_k, w_v, cot)


def spread_kernel(ids, returned, rows, gqw, out_ref, rows_ref, gqw_ref):
    rows_ref[...] = rows[...]
    gqw_ref[...] = gqw[...]
    out_ref[...] = jnp.zeros_like(out_ref)
    for s in range(ids.shape[0]):
        passage = ids[s]

        @pl.when(passage >= 0)
        def _():
            span = rows_at(passage, PLEN)
            out_ref[span, :] += returned[s].astype(F32)


def spread(ids, returned, grad_rows, grad_query_weight, rows):
    vmem = pl.BlockSpec(memory_space=pltpu.VMEM)
    return pl.pallas_call(
        spread_kernel,
        out_shape=(
            jax.ShapeDtypeStruct((rows, returned.shape[2]), F32),
            jax.ShapeDtypeStruct(grad_rows.shape, F32),
            jax.ShapeDtypeStruct(grad_query_weight.shape, F32),
        ),
        in_specs=[pl.BlockSpec(memory_space=pltpu.SMEM), vmem, vmem, vmem],
        out_specs=(vmem, vmem, vmem),
        compiler_params=pltpu.CompilerParams(vmem_limit_bytes=60 << 20),
        name="spread",
    )(ids, returned, grad_rows, grad_query_weight)


def shards(normed, store, passage_ids, w_query, w_gate, w_key, w_value, cotangent):
    grad_rows, returned, grad_query_weight, served_ids = main_call(
        lax.axis_size("st"), lax.axis_size("tp"), passage_ids.T,
        store.reshape(-1, PLEN, store.shape[1]), normed, w_query, w_gate, w_key, w_value, cotangent,
    )
    grad_store, grad_rows, grad_query_weight = spread(
        served_ids, returned, grad_rows, grad_query_weight, store.shape[0]
    )
    return (grad_rows, grad_store, grad_query_weight)


def solution(mesh):
    placed = (
        P("st", None),
        P("st", None),
        P("st", None),
        P(None, "tp"),
        P(None, "tp"),
        P(None, "tp"),
        P(None, "tp"),
        P("st", "tp"),
    )
    return jax.shard_map(
        shards,
        mesh=mesh,
        in_specs=placed,
        out_specs=(P("st", "tp"), P("st", "tp"), P("st", "tp")),
        check_vma=False,
    )
```

time: 90 us -> 69.3 us (0.77)
  blocking collectives: 9.66 us -> 0 us
  Pallas kernels: 75.9 us -> 68.5 us
  other arithmetic: 1.98 us -> 0 us
  local copies, waits for them, and re-layouts: 1.54 us -> 0 us
    all_to_all x1 -> x0, blocking collectives: 9.66 us -> none  [shards(): lax.all_to_all(slot_table.reshape(peer_count, slot_most), 'st', split_axi...]
    pallas_call x2 -> x1, Pallas kernels: 72.5 us -> 65.2 us  [main_call(): pl.pallas_call(functools.partial(main_kernel, st_n, tp_n, reads, slots, p...]
where the time goes in v1:
time: 69.3 us; the launch traced here: 69.2 us
  Pallas kernels  68.5 us (99%)
    pallas_call x1, Pallas kernels, main_call(): pl.pallas_call(functools.partial(main_kernel, st_n, tp_n, reads, slots, p...  65.2 us
    pallas_call x1, Pallas kernels, spread(): pl.pallas_call(spread_kernel, out_shape=(jax.ShapeDtypeStruct((rows, retu...  3.37 us

profile of v1, /device:TPU:0, one launch (start us, length us, event | category | flops | bytes accessed | tf_op | source)
XLA Modules:
  0.0 69.2 jit_solution(14998199451848745727)
XLA Ops:
  0.6 65.2 %main.1 = (f32[512,256]{1,0:T(8,128)}, bf16[16,64,256]{2,1,0:T(8,128)(2,1)}, f32[512,256]{1,0:T(8,128)}, s32[16]{0:T(128)}) custom-call(s32[2,4]{1,0:T(2,128)} %bitcast.3, bf16[32,64,2048]{2,1,0:T(8,128)(2,1)} %bitcast.2, bf16[512,2048]{1,0:T(8,128)(2,1)} %normed_h.1, bf16[2048,256]{1,0:T(8,128)(2,1)} %w_q_h.1, bf16[2048,256]{1,0:T(8,128)(2,1)} %w_g_h.1, ...), custom_call_target="tpu_custom_call" | custom-call | tf_op jit(solution)/shard_map/main/pallas_call | solution.py:430
  65.8 3.4 %spread.1 = (f32[2048,256]{1,0:T(8,128)}, f32[512,256]{1,0:T(8,128)}, f32[512,256]{1,0:T(8,128)}) custom-call(s32[16]{0:T(128)} %get-tuple-element.10.ids, bf16[16,64,256]{2,1,0:T(8,128)(2,1)} %get-tuple-element.11.returned, f32[512,256]{1,0:T(8,128)} %get-tuple-element.12.rows, f32[512,256]{1,0:T(8,128)} %get-tuple-element.13.gqw), custom_call_target="tpu_custom_call" | custom-call | tf_op jit(solution)/shard_map/spread/pallas_call | solution.py:486

commit v2 on v1

v2 whole, which is shorter than its diff:
```python
import functools

import jax
import jax.numpy as jnp
from jax import lax
from jax.experimental import pallas as pl
from jax.experimental.pallas import tpu as pltpu
from jax.sharding import PartitionSpec as P

DH = 128
BLK = 128
PLEN = 64
GROUP = 4
CORES = 2
F32 = jnp.float32
BF16 = jnp.bfloat16
MESH = pl.DeviceIdType.MESH


def dot_nn(a, b):
    return lax.dot_general(a, b, (((1,), (0,)), ((), ())), preferred_element_type=F32)


def dot_nt(a, b):
    return lax.dot_general(a, b, (((1,), (1,)), ((), ())), preferred_element_type=F32)


def dot_tn(a, b):
    return lax.dot_general(a, b, (((0,), (0,)), ((), ())), preferred_element_type=F32)


def rows_at(index, size):
    return pl.ds(pl.multiple_of(index * size, size), size)


def main_kernel(
    st_n, tp_n, reads, slots, pass_dev,
    ids, store_h, normed_h, w_q_h, w_g_h, w_k_h, w_v_h, cot_h,
    rows_out, ret_out, gqw_out, served_out,
    store, normed, w_q, w_g, w_k, w_v, cot, load_sem,
    mine, tables, served_ids, req_of, slot_of, early_of, t_ss, t_rs,
    served, arr_e, arr_all, q_s, gate_s, dq_s, dg_s, dp_s,
    x_out, x_in, z_out, up_in, dn_in, own, part, r_out, r_in, g_out, g_in, g_own,
    kv_ss, kv_rs, x_ss, x_rs, z_ss, z_rs, r_ss, r_rs, g_ss, g_rs, out_sem,
):
    me_st, me_tp = lax.axis_index("st"), lax.axis_index("tp")
    z_n = tp_n // CORES
    me_z, me_c = me_tp // CORES, me_tp % CORES
    mate = (me_st, me_z * CORES + 1 - me_c)
    tok, hw = cot.shape
    depth = w_q.shape[0]
    heads = hw // DH
    blocks = tok // BLK
    cw = depth // tp_n
    first = min(reads, slots)
    n_pos = blocks * reads
    scale = DH ** (-0.5)

    def st_peer(d):
        return lax.rem(me_st + d, st_n)

    def st_from(d):
        return lax.rem(me_st + st_n - d, st_n)

    def load(i, far, near):
        copy = pltpu.make_async_copy(far, near, load_sem.at[i])
        copy.start()
        return copy

    loads_a = [
        load(i, far, near)
        for i, (far, near) in enumerate(((w_k_h, w_k), (store_h, store), (w_v_h, w_v)))
    ]

    above, below = me_z < z_n - 1, me_z > 0
    barrier = pltpu.get_barrier_semaphore()

    def greet(device):
        pl.semaphore_signal(barrier, inc=1, device_id=device, device_id_type=MESH)

    for d in range(1, st_n):
        for c in range(CORES):
            greet((st_peer(d), me_z * CORES + c))

    @pl.when(above)
    def _():
        greet((me_st, (me_z + 1) * CORES + me_c))

    @pl.when(below)
    def _():
        greet((me_st, (me_z - 1) * CORES + me_c))

    greet(mate)

    passages = [ids[i % reads, i // reads] for i in range(n_pos)]
    owners = [lax.div(p, jnp.int32(pass_dev)) for p in passages]
    ranks = []
    for i in range(n_pos):
        rank = jnp.int32(0)
        for j in range(i):
            rank = rank + jnp.where(owners[j] == owners[i], 1, 0)
        ranks.append(rank)
    places = [owners[i] * slots + ranks[i] for i in range(n_pos)]
    for i in range(n_pos):
        slot_of[i] = places[i]
        early_of[i] = owners[i] * first + jnp.minimum(ranks[i], first - 1)
    for s in range(st_n * slots):
        local, position = jnp.int32(-1), jnp.int32(0)
        for i in range(n_pos):
            hit = places[i] == s
            local = jnp.where(hit, passages[i] - (s // slots) * pass_dev, local)
            position = jnp.where(hit, i, position)
        mine[s] = local
        req_of[s] = position

    def barrier_wait():
        pl.semaphore_wait(
            barrier, CORES * (st_n - 1) + 1 + jnp.where(above, 1, 0) + jnp.where(below, 1, 0)
        )

    barrier_wait()

    def remote(src, dst, ss, rs, dev):
        return pltpu.make_async_remote_copy(
            src_ref=src, dst_ref=dst, send_sem=ss, recv_sem=rs, device_id=dev, device_id_type=MESH
        )

    def landed(ref, rs):
        remote(ref, ref, out_sem.at[0], rs, mate).wait_recv()

    def gone(ref, ss):
        remote(ref, ref, ss, out_sem.at[0], mate).wait_send()

    def table_copy(d, c):
        return remote(
            mine, tables.at[d], t_ss.at[c], t_rs.at[0], (st_peer(d), me_z * CORES + c)
        )

    @pl.when(me_c == CORES - 1)
    def _():
        for c in range(CORES):
            for d in range(1, st_n):
                table_copy(d, c).start()

    loads_b = [
        load(3 + i, far, near)
        for i, (far, near) in enumerate(
            ((normed_h, normed), (w_q_h, w_q), (w_g_h, w_g), (cot_h, cot))
        )
    ]

    def store_wait():
        for copy in loads_a:
            copy.wait()

    def table_wait():
        landed(tables.at[:st_n - 1], t_rs.at[0])

    store_wait()
    table_wait()

    def wanted(d, k):
        at = me_st * slots + k
        return tables[st_n - d, at] if d else mine[at]

    dists = list(range(1, st_n)) + [0]
    halves = (0, 1)

    def kv_copy(d, k):
        landing = arr_e.at[me_st * first + k] if k < first else arr_all.at[me_st * slots + k]
        source = served.at[d * slots + k]
        late = 0 if k < first else 1
        return remote(source, landing, kv_ss.at[late], kv_rs.at[late], (st_peer(d), me_tp))

    def project(k, some):
        rows = jnp.concatenate([store[jnp.maximum(wanted(d, k), 0)] for d in some], axis=0)
        for half in halves:
            made = dot_nn(rows, (w_k, w_v)[half][...]).astype(BF16)
            for i, d in enumerate(some):
                piece = made[i * PLEN:(i + 1) * PLEN]
                if d:
                    served[d * slots + k, half] = piece
                elif k < first:
                    arr_e[me_st * first + k, half] = piece
                else:
                    arr_all[me_st * slots + k, half] = piece
        if k < first:
            for d in some:
                if d:
                    kv_copy(d, k).start()

    for k in range(slots):
        for i in range(0, st_n, GROUP):
            project(k, dists[i:i + GROUP])

    for d in range(st_n):
        for k in range(slots):
            served_ids[st_peer(d) * slots + k] = wanted(d, k)

    outs = []

    def put(i, near, far):
        copy = pltpu.make_async_copy(near, far, out_sem.at[i])
        copy.start()
        outs.append(copy)

    put(2, served_ids, served_out)
    for copy in loads_b:
        copy.wait()
    tile = 2 * BLK

    @pl.loop(0, tok // tile)
    def _(i):
        span = rows_at(i, tile)
        q_s[span, :] = dot_nn(normed[span, :], w_q[...]).astype(BF16)
        gate_s[span, :] = jax.nn.sigmoid(dot_nn(normed[span, :], w_g[...]))

    late = (st_n - 1) * (slots - first)

    def kv_arrived(phase):
        if phase == 0:
            landed(arr_e.at[:(st_n - 1) * first], kv_rs.at[0])
        else:
            landed(arr_all.at[:late], kv_rs.at[1])

    span = reads * PLEN

    def attend(b):
        if b == 0 or slots == first:
            parts = [arr_e[early_of[b * reads + r]] for r in range(reads)]
        else:
            parts = [arr_all[slot_of[b * reads + r]] for r in range(reads)]
        keys = jnp.concatenate([part[0] for part in parts], axis=0)
        values = jnp.concatenate([part[1] for part in parts], axis=0)
        toks = slice(b * BLK, (b + 1) * BLK)
        ctx = slice(b * span, (b + 1) * span)
        for h in range(heads):
            ch = slice(h * DH, (h + 1) * DH)
            chv = slice(hw + h * DH, hw + (h + 1) * DH)
            k, v = keys[:, ch], values[:, ch]
            q = q_s[toks, ch]
            gate = gate_s[toks, ch]
            up = cot[toks, ch].astype(F32)
            d_att = (up * gate).astype(BF16)
            d_p = dot_nt(d_att, v)
            s = dot_nt(q, k) * scale
            e = jnp.exp(s - jnp.max(s, axis=1, keepdims=True))
            p = e / jnp.sum(e, axis=1, keepdims=True)
            low = p.astype(BF16)
            att = dot_nn(low, v)
            dg_s[toks, ch] = (up * att * gate * (1.0 - gate)).astype(BF16)
            dp_s[ctx, chv] = dot_tn(low, d_att).astype(BF16)
            delta = jnp.sum(d_p * p, axis=1, keepdims=True)
            d_s = (p * (d_p - delta) * scale).astype(BF16)
            dq_s[toks, ch] = dot_nn(d_s, k).astype(BF16)
            dp_s[ctx, ch] = dot_tn(d_s, q).astype(BF16)

    def chunk(g, t):
        which, b = g
        w_rows = rows_at(t, cw)
        if which == 0:
            ctx = slice(b * span, (b + 1) * span)
            return dot_nt(dp_s[ctx, :hw], w_k[w_rows, :]) + dot_nt(dp_s[ctx, hw:], w_v[w_rows, :])
        toks = slice(b * BLK, (b + 1) * BLK)
        return dot_nt(dq_s[toks, :], w_q[w_rows, :]) + dot_nt(dg_s[toks, :], w_g[w_rows, :])

    order = []
    for i in range((z_n + 1) // 2):
        order += [z_n - 1 - i, i] if z_n - 1 - i != i else [i]

    def piece_of(g, t):
        return (g[0] * blocks + g[1]) * z_n + t

    def all_of(g):
        at = piece_of(g, 0)
        return slice(at, at + z_n)

    batches = [[(0, 0)], [(1, 0)]] + [[(0, b)] for b in range(1, blocks)]
    batches.append([(1, b) for b in range(1, blocks)])
    early_groups = [g for batch in batches[:-1] for g in batch]

    def hop(g, t, up):
        n = piece_of(g, t)
        to = me_z + 1 if up else me_z - 1
        return remote(
            z_out.at[n], (up_in if up else dn_in).at[n],
            z_ss.at[0 if g in early_groups else 1],
            z_rs.at[piece_of(g, 0) // z_n * (z_n + 1) + t + (1 if up else 0)],
            (me_st, to * CORES + me_c),
        )

    def give(g):
        for t in order:
            x_out[piece_of(g, t)] = chunk(g, t * CORES + 1 - me_c).astype(BF16)
        i = piece_of(g, 0) // z_n
        for t in order:
            n = piece_of(g, t)
            remote(x_out.at[n], x_in.at[n], x_ss.at[i], x_rs.at[i], mate).start()

    def take(g):
        for t in order:
            own[piece_of(g, t)] = chunk(g, t * CORES + me_c)
        landed(x_in.at[all_of(g)], x_rs.at[piece_of(g, 0) // z_n])
        for t in order:
            n = piece_of(g, t)
            own[n] = own[n] + x_in[n].astype(F32)

    def depart(batch):
        @pl.when(me_z == 0)
        def _():
            for t in range(z_n - 1, 0, -1):
                for g in batch:
                    n = piece_of(g, t)
                    z_out[n] = own[n].astype(BF16)
                    hop(g, t, True).start()

        @pl.when(me_z == z_n - 1)
        def _():
            for t in range(z_n - 1):
                for g in batch:
                    n = piece_of(g, t)
                    z_out[n] = own[n].astype(BF16)
                    hop(g, t, False).start()

    def pass_on(batch, up, t):
        landing = up_in if up else dn_in
        for g in batch:
            n = piece_of(g, t)
            hop(g, t, up).wait_recv()
            z_out[n] = (own[n] + landing[n].astype(F32)).astype(BF16)
            hop(g, t, up).start()

    def relay(batch, z, stages):
        moves = [(z_n - 1 - t, z, True, t) for t in range(z + 1, z_n)]
        moves += [(t, z_n - 1 - z, False, t) for t in range(z)]
        moves = [m for m in moves if m[1] in stages]

        @pl.when(me_z == z)
        def _():
            for m in sorted(moves, key=lambda m: (m[0] + m[1], -m[1])):
                pass_on(batch, m[2], m[3])

    def gathered(g):
        n = piece_of(g, me_z)

        @pl.when(below)
        def _():
            hop(g, me_z, True).wait_recv()
            own[n] = own[n] + up_in[n].astype(F32)

        @pl.when(above)
        def _():
            hop(g, me_z, False).wait_recv()
            own[n] = own[n] + dn_in[n].astype(F32)

        which, b = g
        if which == 0:
            part[b * reads:(b + 1) * reads] = own[n].astype(BF16).reshape(reads, PLEN, cw)

    reads_end = blocks
    relayed = [0]

    def relay_step():
        j = relayed[0]
        relayed[0] += 1
        for z in range(1, z_n - 1):
            for k in range(1, z_n - 1):
                if 0 <= j - (k - 1) <= reads_end and k in (z, z_n - 1 - z):
                    relay(batches[j - (k - 1)], z, (k,))

    kv_arrived(0)
    for k in range(first, slots):
        for d in range(1, st_n):
            kv_copy(d, k).start()
    attend(0)
    give((0, 0))
    take((0, 0))
    depart(batches[0])
    give((1, 0))
    take((1, 0))
    depart(batches[1])
    if slots > first:
        for o in range(st_n):
            for k in range(first):
                arr_all[o * slots + k] = arr_e[o * first + k]
        kv_arrived(1)

    for b in range(1, blocks):
        attend(b)
        give((0, b))
        if b > 1:
            take((0, b - 1))
            depart([(0, b - 1)])
        if b == 2:
            relay_step()
    for b in range(1, blocks):
        give((1, b))
        if b == 1:
            take((0, blocks - 1))
            depart([(0, blocks - 1)])
            relay_step()
        else:
            take((1, b - 1))
    take((1, blocks - 1))
    depart(batches[-1])
    relay_step()

    dw = depth // st_n
    for d in list(range(1, st_n)) + [0]:
        term = dot_tn(normed[:, rows_at(st_peer(d), dw)], dq_s[...])
        if d == 0:
            g_own[...] = term
        else:
            g_out[d] = term.astype(BF16)
            remote(
                g_out.at[d], g_in.at[d], g_ss.at[0], g_rs.at[0], (st_peer(d), me_tp)
            ).start()

    while relayed[0] < reads_end + 1 + max(z_n - 3, 0):
        relay_step()
    for b in range(blocks):
        gathered((0, b))
    for s in range(st_n * slots):
        r_out[s] = part[req_of[s]]
    for d in range(1, st_n):
        remote(
            r_out.at[rows_at(st_peer(d), slots)], r_in.at[rows_at(me_st, slots)],
            r_ss.at[0], r_rs.at[0], (st_peer(d), me_tp),
        ).start()
    r_in[rows_at(me_st, slots)] = r_out[rows_at(me_st, slots)]

    def gqw_wait():
        total = g_own[...]
        landed(g_in.at[:st_n - 1], g_rs.at[0])
        for d in range(1, st_n):
            total = total + g_in[d].astype(F32)
        g_own[...] = total
        put(1, g_own, gqw_out)

    def send_wait():
        gone(served.at[:(st_n - 1) * first], kv_ss.at[0])
        if slots > first:
            gone(served.at[:late], kv_ss.at[1])
        for g in [g for batch in batches for g in batch]:
            gone(x_out.at[all_of(g)], x_ss.at[piece_of(g, 0) // z_n])
        gone(g_out.at[:st_n - 1], g_ss.at[0])
        gone(z_out.at[:len(early_groups) * (z_n - 1)], z_ss.at[0])

    @pl.when(me_c == CORES - 1)
    def _():
        for c in range(CORES):
            gone(tables.at[:st_n - 1], t_ss.at[c])

    for z in range(1, z_n - 1):
        relay(batches[-1], z, range(z_n))
    gqw_wait()
    send_wait()

    def ret_wait():
        landed(r_in.at[:(st_n - 1) * slots], r_rs.at[0])
        put(0, r_in, ret_out)

    ret_wait()
    for b in range(blocks):
        gathered((1, b))
        put(3 + b, own.at[piece_of((1, b), me_z)], rows_out.at[b * BLK:(b + 1) * BLK])
    gone(z_out.at[:len(batches[-1]) * (z_n - 1)], z_ss.at[1])
    gone(r_out.at[:(st_n - 1) * slots], r_ss.at[0])

    def out_wait():
        for copy in outs:
            copy.wait()

    out_wait()


def main_call(st_n, tp_n, ids, store, normed, w_q, w_g, w_k, w_v, cot):
    reads, blocks = ids.shape
    tok, hw = cot.shape
    depth = w_q.shape[0]
    cw, dw, z_n = depth // tp_n, depth // st_n, tp_n // CORES
    pass_dev = store.shape[0]
    n_pos = blocks * reads
    slots = max(1, 2 * n_pos // st_n)
    first = min(reads, slots)
    ctx = blocks * reads * PLEN
    slot_total = st_n * slots
    hbm = pl.BlockSpec(memory_space=pl.ANY)
    smem = pl.BlockSpec(memory_space=pltpu.SMEM)
    pieces = 2 * blocks * z_n
    piece = lambda kind=BF16: pltpu.VMEM((pieces, BLK, cw), kind)
    sem = lambda n: pltpu.SemaphoreType.DMA((n,))
    table = lambda *n: pltpu.SMEM(n, jnp.int32)
    assert ctx == tok
    return pl.pallas_call(
        functools.partial(main_kernel, st_n, tp_n, reads, slots, pass_dev),
        out_shape=(
            jax.ShapeDtypeStruct((tok, cw), F32),
            jax.ShapeDtypeStruct((slot_total, PLEN, cw), BF16),
            jax.ShapeDtypeStruct((dw, hw), F32),
            jax.ShapeDtypeStruct((slot_total,), jnp.int32),
        ),
        in_specs=[smem] + [hbm] * 7,
        out_specs=(hbm, hbm, hbm, hbm),
        scratch_shapes=[
            *[pltpu.VMEM(a.shape, a.dtype) for a in (store, normed, w_q, w_g, w_k, w_v, cot)],
            sem(7),
            table(slot_total), table(st_n, slot_total), table(slot_total),
            table(slot_total), table(n_pos), table(n_pos),
            sem(CORES), sem(1),
            pltpu.VMEM((slot_total, 2, PLEN, hw), BF16),
            pltpu.VMEM((st_n * first, 2, PLEN, hw), BF16),
            pltpu.VMEM((slot_total, 2, PLEN, hw), BF16),
            pltpu.VMEM((tok, hw), BF16),
            pltpu.VMEM((tok, hw), F32),
            pltpu.VMEM((tok, hw), BF16),
            pltpu.VMEM((tok, hw), BF16),
            pltpu.VMEM((ctx, 2 * hw), BF16),
            piece(), piece(), piece(), piece(), piece(), piece(F32),
            pltpu.VMEM((ctx // PLEN, PLEN, cw), BF16),
            pltpu.VMEM((slot_total, PLEN, cw), BF16),
            pltpu.VMEM((slot_total, PLEN, cw), BF16),
            pltpu.VMEM((st_n, dw, hw), BF16),
            pltpu.VMEM((st_n, dw, hw), BF16),
            pltpu.VMEM((dw, hw), F32),
            sem(2), sem(2), sem(2 * blocks), sem(2 * blocks), sem(2), sem(2 * blocks * (z_n + 1)),
            sem(1), sem(1), sem(1), sem(1), sem(3 + blocks),
        ],
        compiler_params=pltpu.CompilerParams(
            collective_id=0, has_side_effects=True, vmem_limit_bytes=62 << 20
        ),
        name="main",
    )(ids, store, normed, w_q, w_g, w_k, w_v, cot)


def spread_kernel(
    ids_h, returned_h, rows_h, gqw_h, out_h, rows_out, gqw_out,
    ids, returned, rows, gqw, total, in_sem, out_sem, chunk_sem,
):
    slots, passes = ids.shape[0], out_h.shape[0]
    names = pltpu.make_async_copy(ids_h, ids, in_sem.at[3])
    names.start()
    pull = pltpu.make_async_copy(returned_h, returned, in_sem.at[2])
    pull.start()
    sides, loads = [], []
    for i, (far, near, out) in enumerate(((rows_h, rows, rows_out), (gqw_h, gqw, gqw_out))):
        loads.append(pltpu.make_async_copy(far, near, in_sem.at[i]))
        loads[-1].start()
        sides.append(pltpu.make_async_copy(near, out, out_sem.at[i]))
    total[...] = jnp.zeros_like(total)
    names.wait()
    pull.wait()
    for s in range(slots):

        @pl.when(ids[s] >= 0)
        def _():
            total[ids[s]] += returned[s].astype(F32)

    chunks = chunk_sem.shape[0]
    size = passes // chunks
    for i in range(chunks):
        span = slice(i * size, (i + 1) * size)
        sides.append(pltpu.make_async_copy(total.at[span], out_h.at[span], chunk_sem.at[i]))
        sides[-1].start()
    for load, store in zip(loads, sides):
        load.wait()
        store.start()
    for copy in sides:
        copy.wait()


def spread(ids, returned, grad_rows, grad_query_weight, passes):
    width = returned.shape[2]
    hbm = pl.BlockSpec(memory_space=pl.ANY)
    chunks = GROUP if passes % GROUP == 0 else 1
    return pl.pallas_call(
        spread_kernel,
        out_shape=(
            jax.ShapeDtypeStruct((passes, PLEN, width), F32),
            jax.ShapeDtypeStruct(grad_rows.shape, F32),
            jax.ShapeDtypeStruct(grad_query_weight.shape, F32),
        ),
        in_specs=[hbm] * 4,
        out_specs=(hbm,) * 3,
        scratch_shapes=[
            pltpu.SMEM(ids.shape, jnp.int32),
            pltpu.VMEM(returned.shape, BF16),
            pltpu.VMEM(grad_rows.shape, F32),
            pltpu.VMEM(grad_query_weight.shape, F32),
            pltpu.VMEM((passes, PLEN, width), F32),
            pltpu.SemaphoreType.DMA((4,)),
            pltpu.SemaphoreType.DMA((2,)),
            pltpu.SemaphoreType.DMA((chunks,)),
        ],
        compiler_params=pltpu.CompilerParams(vmem_limit_bytes=62 << 20),
        name="spread",
    )(ids, returned, grad_rows, grad_query_weight)


def shards(normed, store, passage_ids, w_query, w_gate, w_key, w_value, cotangent):
    grad_rows, returned, grad_query_weight, served_ids = main_call(
        lax.axis_size("st"), lax.axis_size("tp"), passage_ids.T,
        store.reshape(-1, PLEN, store.shape[1]), normed, w_query, w_gate, w_key, w_value, cotangent,
    )
    grad_store, grad_rows, grad_query_weight = spread(
        served_ids, returned, grad_rows, grad_query_weight, store.shape[0] // PLEN
    )
    return (grad_rows, grad_store.reshape(store.shape[0], -1), grad_query_weight)


def solution(mesh):
    placed = (
        P("st", None),
        P("st", None),
        P("st", None),
        P(None, "tp"),
        P(None, "tp"),
        P(None, "tp"),
        P(None, "tp"),
        P("st", "tp"),
    )
    return jax.shard_map(
        shards,
        mesh=mesh,
        in_specs=placed,
        out_specs=(P("st", "tp"), P("st", "tp"), P("st", "tp")),
        check_vma=False,
    )
```

time: 69.3 us -> 59.5 us (0.86); the launches traced: 69.2 us -> 58.4 us
  Pallas kernels: 68.5 us -> 57.7 us
    pallas_call x1, Pallas kernels: 65.2 us -> 54.8 us  [main_call(): pl.pallas_call(functools.partial(main_kernel, st_n, tp_n, reads, slots, p...]
where the time goes in v2:
time: 59.5 us; the launch traced here: 58.4 us
  Pallas kernels  57.7 us (97%)
  between operations  0.64 us (1%)
    pallas_call x1, Pallas kernels, main_call(): pl.pallas_call(functools.partial(main_kernel, st_n, tp_n, reads, slots, p...  54.8 us
    pallas_call x1, Pallas kernels, spread(): pl.pallas_call(spread_kernel, out_shape=(jax.ShapeDtypeStruct((passes, PL...  2.96 us

profile of v2, /device:TPU:0, one launch (start us, length us, event | category | flops | bytes accessed | tf_op | source)
XLA Modules:
  0.0 58.4 jit_solution(13955396205391455943)
XLA Ops:
  0.6 54.8 %main.1 = (f32[512,256]{1,0:T(8,128)}, bf16[16,64,256]{2,1,0:T(8,128)(2,1)}, f32[512,256]{1,0:T(8,128)}, s32[16]{0:T(128)}) custom-call(s32[2,4]{1,0:T(2,128)} %bitcast.4, bf16[32,64,2048]{2,1,0:T(8,128)(2,1)} %bitcast.3, bf16[512,2048]{1,0:T(8,128)(2,1)} %normed_h.1, bf16[2048,256]{1,0:T(8,128)(2,1)} %w_q_h.1, bf16[2048,256]{1,0:T(8,128)(2,1)} %w_g_h.1, ...), custom_call_target="tpu_custom_call" | custom-call | tf_op jit(solution)/shard_map/main/pallas_call | solution.py:495
  55.4 3.0 %spread.1 = (f32[32,64,256]{2,1,0:T(8,128)}, f32[512,256]{1,0:T(8,128)}, f32[512,256]{1,0:T(8,128)}) custom-call(s32[16]{0:T(128)} %get-tuple-element.10.ids_h, bf16[16,64,256]{2,1,0:T(8,128)(2,1)} %get-tuple-element.11.returned_h, f32[512,256]{1,0:T(8,128)} %get-tuple-element.12.rows_h, f32[512,256]{1,0:T(8,128)} %get-tuple-element.13.gqw_h), custom_call_target="tpu_custom_call" | custom-call | tf_op jit(solution)/shard_map/spread/pallas_call | solution.py:576

commit v3 on v2

--- a/solution.py
+++ b/solution.py
@@ -35,10 +35,10 @@
 
 def main_kernel(
     st_n, tp_n, reads, slots, pass_dev,
-    ids, store_h, normed_h, w_q_h, w_g_h, w_k_h, w_v_h, cot_h,
+    ids_h, store_h, normed_h, w_q_h, w_g_h, w_k_h, w_v_h, cot_h,
     rows_out, ret_out, gqw_out, served_out,
     store, normed, w_q, w_g, w_k, w_v, cot, load_sem,
-    mine, tables, served_ids, req_of, slot_of, early_of, t_ss, t_rs,
+    ids, mine, tables, served_ids, req_of, slot_of, early_of, t_ss, t_rs,
     served, arr_e, arr_all, q_s, gate_s, dq_s, dg_s, dp_s,
     x_out, x_in, z_out, up_in, dn_in, own, part, r_out, r_in, g_out, g_in, g_own,
     kv_ss, kv_rs, x_ss, x_rs, z_ss, z_rs, r_ss, r_rs, g_ss, g_rs, out_sem,
@@ -67,6 +67,7 @@
         copy.start()
         return copy
 
+    ids_load = load(7, ids_h, ids)
     loads_a = [
         load(i, far, near)
         for i, (far, near) in enumerate(((w_k_h, w_k), (store_h, store), (w_v_h, w_v)))
@@ -92,6 +93,7 @@
 
     greet(mate)
 
+    ids_load.wait()
     passages = [ids[i % reads, i // reads] for i in range(n_pos)]
     owners = [lax.div(p, jnp.int32(pass_dev)) for p in passages]
     ranks = []
@@ -163,7 +165,6 @@
         at = me_st * slots + k
         return tables[st_n - d, at] if d else mine[at]
 
-    dists = list(range(1, st_n)) + [0]
     halves = (0, 1)
 
     def kv_copy(d, k):
@@ -172,11 +173,11 @@
         late = 0 if k < first else 1
         return remote(source, landing, kv_ss.at[late], kv_rs.at[late], (st_peer(d), me_tp))
 
-    def project(k, some):
-        rows = jnp.concatenate([store[jnp.maximum(wanted(d, k), 0)] for d in some], axis=0)
+    def project(some):
+        rows = jnp.concatenate([store[jnp.maximum(wanted(d, k), 0)] for d, k in some], axis=0)
         for half in halves:
             made = dot_nn(rows, (w_k, w_v)[half][...]).astype(BF16)
-            for i, d in enumerate(some):
+            for i, (d, k) in enumerate(some):
                 piece = made[i * PLEN:(i + 1) * PLEN]
                 if d:
                     served[d * slots + k, half] = piece
@@ -184,14 +185,17 @@
                     arr_e[me_st * first + k, half] = piece
                 else:
                     arr_all[me_st * slots + k, half] = piece
-        if k < first:
-            for d in some:
-                if d:
-                    kv_copy(d, k).start()
-
-    for k in range(slots):
-        for i in range(0, st_n, GROUP):
-            project(k, dists[i:i + GROUP])
+        for d, k in some:
+            if d and k < first:
+                kv_copy(d, k).start()
+
+    far = [(d, k) for k in range(slots) for d in range(1, st_n)]
+    size = st_n - 1 if st_n <= GROUP else GROUP
+    for i in range(0, len(far), size):
+        project(far[i:i + size])
+    near = [(0, k) for k in range(slots)]
+    for i in range(0, slots, GROUP):
+        project(near[i:i + GROUP])
 
     for d in range(st_n):
         for k in range(slots):
@@ -234,26 +238,32 @@
         values = jnp.concatenate([part[1] for part in parts], axis=0)
         toks = slice(b * BLK, (b + 1) * BLK)
         ctx = slice(b * span, (b + 1) * span)
-        for h in range(heads):
-            ch = slice(h * DH, (h + 1) * DH)
-            chv = slice(hw + h * DH, hw + (h + 1) * DH)
-            k, v = keys[:, ch], values[:, ch]
-            q = q_s[toks, ch]
-            gate = gate_s[toks, ch]
-            up = cot[toks, ch].astype(F32)
-            d_att = (up * gate).astype(BF16)
-            d_p = dot_nt(d_att, v)
-            s = dot_nt(q, k) * scale
-            e = jnp.exp(s - jnp.max(s, axis=1, keepdims=True))
-            p = e / jnp.sum(e, axis=1, keepdims=True)
-            low = p.astype(BF16)
-            att = dot_nn(low, v)
-            dg_s[toks, ch] = (up * att * gate * (1.0 - gate)).astype(BF16)
-            dp_s[ctx, chv] = dot_tn(low, d_att).astype(BF16)
-            delta = jnp.sum(d_p * p, axis=1, keepdims=True)
-            d_s = (p * (d_p - delta) * scale).astype(BF16)
-            dq_s[toks, ch] = dot_nn(d_s, k).astype(BF16)
-            dp_s[ctx, ch] = dot_tn(d_s, q).astype(BF16)
+        cols = [slice(h * DH, (h + 1) * DH) for h in range(heads)]
+        colsv = [slice(hw + h * DH, hw + (h + 1) * DH) for h in range(heads)]
+        k = [keys[:, ch] for ch in cols]
+        v = [values[:, ch] for ch in cols]
+        q = [q_s[toks, ch] for ch in cols]
+        gate = [gate_s[toks, ch] for ch in cols]
+        up = [cot[toks, ch].astype(F32) for ch in cols]
+        each = range(heads)
+        s = [dot_nt(q[h], k[h]) * scale for h in each]
+        d_att = [(up[h] * gate[h]).astype(BF16) for h in each]
+        d_p = [dot_nt(d_att[h], v[h]) for h in each]
+        e = [jnp.exp(s[h] - jnp.max(s[h], axis=1, keepdims=True)) for h in each]
+        p = [e[h] / jnp.sum(e[h], axis=1, keepdims=True) for h in each]
+        low = [p[h].astype(BF16) for h in each]
+        delta = [jnp.sum(d_p[h] * p[h], axis=1, keepdims=True) for h in each]
+        d_s = [(p[h] * (d_p[h] - delta[h]) * scale).astype(BF16) for h in each]
+        d_k = [dot_tn(d_s[h], q[h]) for h in each]
+        d_v = [dot_tn(low[h], d_att[h]) for h in each]
+        att = [dot_nn(low[h], v[h]) for h in each]
+        d_q = [dot_nn(d_s[h], k[h]) for h in each]
+        for h in each:
+            dp_s[ctx, cols[h]] = d_k[h].astype(BF16)
+            dp_s[ctx, colsv[h]] = d_v[h].astype(BF16)
+        for h in each:
+            dg_s[toks, cols[h]] = (up[h] * att[h] * gate[h] * (1.0 - gate[h])).astype(BF16)
+            dq_s[toks, cols[h]] = d_q[h].astype(BF16)
 
     def chunk(g, t):
         which, b = g
@@ -486,7 +496,6 @@
     ctx = blocks * reads * PLEN
     slot_total = st_n * slots
     hbm = pl.BlockSpec(memory_space=pl.ANY)
-    smem = pl.BlockSpec(memory_space=pltpu.SMEM)
     pieces = 2 * blocks * z_n
     piece = lambda kind=BF16: pltpu.VMEM((pieces, BLK, cw), kind)
     sem = lambda n: pltpu.SemaphoreType.DMA((n,))
@@ -500,12 +509,12 @@
             jax.ShapeDtypeStruct((dw, hw), F32),
             jax.ShapeDtypeStruct((slot_total,), jnp.int32),
         ),
-        in_specs=[smem] + [hbm] * 7,
+        in_specs=[hbm] * 8,
         out_specs=(hbm, hbm, hbm, hbm),
         scratch_shapes=[
             *[pltpu.VMEM(a.shape, a.dtype) for a in (store, normed, w_q, w_g, w_k, w_v, cot)],
-            sem(7),
-            table(slot_total), table(st_n, slot_total), table(slot_total),
+            sem(8),
+            table(*ids.shape), table(slot_total), table(st_n, slot_total), table(slot_total),
             table(slot_total), table(n_pos), table(n_pos),
             sem(CORES), sem(1),
             pltpu.VMEM((slot_total, 2, PLEN, hw), BF16),
@@ -527,29 +536,29 @@
             sem(1), sem(1), sem(1), sem(1), sem(3 + blocks),
         ],
         compiler_params=pltpu.CompilerParams(
-            collective_id=0, has_side_effects=True, vmem_limit_bytes=62 << 20
+            collective_id=0, has_side_effects=True, vmem_limit_bytes=46 << 20
         ),
         name="main",
-    )(ids, store, normed, w_q, w_g, w_k, w_v, cot)
+    )(*[
+        pltpu.with_memory_space_constraint(a, pltpu.HBM)
+        for a in (ids, store, normed, w_q, w_g, w_k, w_v, cot)
+    ])
 
 
 def spread_kernel(
-    ids_h, returned_h, rows_h, gqw_h, out_h, rows_out, gqw_out,
-    ids, returned, rows, gqw, total, in_sem, out_sem, chunk_sem,
+    ids_h, returned, rows, gqw, out_h, rows_out, gqw_out, ids, total, sems, chunk_sem,
 ):
     slots, passes = ids.shape[0], out_h.shape[0]
-    names = pltpu.make_async_copy(ids_h, ids, in_sem.at[3])
+    names = pltpu.make_async_copy(ids_h, ids, sems.at[2])
     names.start()
-    pull = pltpu.make_async_copy(returned_h, returned, in_sem.at[2])
-    pull.start()
-    sides, loads = [], []
-    for i, (far, near, out) in enumerate(((rows_h, rows, rows_out), (gqw_h, gqw, gqw_out))):
-        loads.append(pltpu.make_async_copy(far, near, in_sem.at[i]))
-        loads[-1].start()
-        sides.append(pltpu.make_async_copy(near, out, out_sem.at[i]))
+    outs = [
+        pltpu.make_async_copy(near, far, sems.at[i])
+        for i, (near, far) in enumerate(((rows, rows_out), (gqw, gqw_out)))
+    ]
+    for copy in outs:
+        copy.start()
     total[...] = jnp.zeros_like(total)
     names.wait()
-    pull.wait()
     for s in range(slots):
 
         @pl.when(ids[s] >= 0)
@@ -560,18 +569,16 @@
     size = passes // chunks
     for i in range(chunks):
         span = slice(i * size, (i + 1) * size)
-        sides.append(pltpu.make_async_copy(total.at[span], out_h.at[span], chunk_sem.at[i]))
-        sides[-1].start()
-    for load, store in zip(loads, sides):
-        load.wait()
-        store.start()
-    for copy in sides:
+        outs.append(pltpu.make_async_copy(total.at[span], out_h.at[span], chunk_sem.at[i]))
+        outs[-1].start()
+    for copy in outs:
         copy.wait()
 
 
 def spread(ids, returned, grad_rows, grad_query_weight, passes):
     width = returned.shape[2]
     hbm = pl.BlockSpec(memory_space=pl.ANY)
+    vmem = pl.BlockSpec(memory_space=pltpu.VMEM)
     chunks = GROUP if passes % GROUP == 0 else 1
     return pl.pallas_call(
         spread_kernel,
@@ -580,19 +587,15 @@
             jax.ShapeDtypeStruct(grad_rows.shape, F32),
             jax.ShapeDtypeStruct(grad_query_weight.shape, F32),
         ),
-        in_specs=[hbm] * 4,
+        in_specs=[hbm] + [vmem] * 3,
         out_specs=(hbm,) * 3,
         scratch_shapes=[
             pltpu.SMEM(ids.shape, jnp.int32),
-            pltpu.VMEM(returned.shape, BF16),
-            pltpu.VMEM(grad_rows.shape, F32),
-            pltpu.VMEM(grad_query_weight.shape, F32),
             pltpu.VMEM((passes, PLEN, width), F32),
-            pltpu.SemaphoreType.DMA((4,)),
-            pltpu.SemaphoreType.DMA((2,)),
+            pltpu.SemaphoreType.DMA((3,)),
             pltpu.SemaphoreType.DMA((chunks,)),
         ],
-        compiler_params=pltpu.CompilerParams(vmem_limit_bytes=62 << 20),
+        compiler_params=pltpu.CompilerParams(vmem_limit_bytes=8 << 20),
         name="spread",
     )(ids, returned, grad_rows, grad_query_weight)
 

time: 59.5 us -> 57.1 us (0.960)
  Pallas kernels: 57.7 us -> 55.8 us
    pallas_call x1, Pallas kernels: 54.8 us -> 53.8 us  [main_call(): pl.pallas_call(functools.partial(main_kernel, st_n, tp_n, reads, slots, p...]
    pallas_call x1, Pallas kernels: 2.96 us -> 2.07 us  [spread(): pl.pallas_call(spread_kernel, out_shape=(jax.ShapeDtypeStruct((passes, PL...]
where the time goes in v3:
time: 57.1 us; the launch traced here: 56.5 us
  Pallas kernels  55.8 us (98%)
  between operations  0.64 us (1%)
    pallas_call x1, Pallas kernels, main_call(): pl.pallas_call(functools.partial(main_kernel, st_n, tp_n, reads, slots, p...  53.8 us
    pallas_call x1, Pallas kernels, spread(): pl.pallas_call(spread_kernel, out_shape=(jax.ShapeDtypeStruct((passes, PL...  2.07 us

profile of v3, /device:TPU:0, one launch (start us, length us, event | category | flops | bytes accessed | tf_op | source)
XLA Modules:
  0.0 56.5 jit_solution(15989273330644105162)
XLA Ops:
  0.6 53.8 %main.1 = (f32[512,256]{1,0:T(8,128)S(1)}, bf16[16,64,256]{2,1,0:T(8,128)(2,1)S(1)}, f32[512,256]{1,0:T(8,128)S(1)}, s32[16]{0:T(128)S(1)}) custom-call(s32[2,4]{1,0:T(2,128)} %bitcast.4, bf16[32,64,2048]{2,1,0:T(8,128)(2,1)} %bitcast.3, bf16[512,2048]{1,0:T(8,128)(2,1)} %normed_h.1, bf16[2048,256]{1,0:T(8,128)(2,1)} %w_q_h.1, bf16[2048,256]{1,0:T(8,128)(2,1)} %w_g_h.1, ...), custom_call_target="tpu_custom_call" | custom-call | tf_op jit(solution)/shard_map/main/pallas_call | solution.py:504
  54.4 2.1 %spread.1 = (f32[32,64,256]{2,1,0:T(8,128)}, f32[512,256]{1,0:T(8,128)}, f32[512,256]{1,0:T(8,128)}) custom-call(s32[16]{0:T(128)S(1)} %get-tuple-element.10.ids_h, bf16[16,64,256]{2,1,0:T(8,128)(2,1)S(1)} %get-tuple-element.11.returned, f32[512,256]{1,0:T(8,128)S(1)} %get-tuple-element.12.rows, f32[512,256]{1,0:T(8,128)S(1)} %get-tuple-element.13.gqw), custom_call_target="tpu_custom_call" | custom-call | tf_op jit(solution)/shard_map/spread/pallas_call | solution.py:583

commit v4 on v3

--- a/solution.py
+++ b/solution.py
@@ -161,9 +161,12 @@
     store_wait()
     table_wait()
 
-    def wanted(d, k):
+    def wanted(i, k):
         at = me_st * slots + k
-        return tables[st_n - d, at] if d else mine[at]
+        return tables[st_n - reach(i), at] if i else mine[at]
+
+    def reach(i):
+        return jnp.where(lax.rem(me_st, 2) == 0, st_n - i, i) if i else 0
 
     halves = (0, 1)
 
@@ -171,7 +174,9 @@
         landing = arr_e.at[me_st * first + k] if k < first else arr_all.at[me_st * slots + k]
         source = served.at[d * slots + k]
         late = 0 if k < first else 1
-        return remote(source, landing, kv_ss.at[late], kv_rs.at[late], (st_peer(d), me_tp))
+        return remote(
+            source, landing, kv_ss.at[late], kv_rs.at[late], (st_peer(reach(d)), me_tp)
+        )
 
     def project(some):
         rows = jnp.concatenate([store[jnp.maximum(wanted(d, k), 0)] for d, k in some], axis=0)
@@ -199,7 +204,7 @@
 
     for d in range(st_n):
         for k in range(slots):
-            served_ids[st_peer(d) * slots + k] = wanted(d, k)
+            served_ids[st_peer(reach(d)) * slots + k] = wanted(d, k)
 
     outs = []
 
@@ -305,7 +310,7 @@
         i = piece_of(g, 0) // z_n
         for t in order:
             n = piece_of(g, t)
-            remote(x_out.at[n], x_in.at[n], x_ss.at[i], x_rs.at[i], mate).start()
+            remote(x_out.at[n], x_in.at[n], x_ss.at[0], x_rs.at[i], mate).start()
 
     def take(g):
         for t in order:
@@ -451,8 +456,7 @@
         gone(served.at[:(st_n - 1) * first], kv_ss.at[0])
         if slots > first:
             gone(served.at[:late], kv_ss.at[1])
-        for g in [g for batch in batches for g in batch]:
-            gone(x_out.at[all_of(g)], x_ss.at[piece_of(g, 0) // z_n])
+        gone(x_out, x_ss.at[0])
         gone(g_out.at[:st_n - 1], g_ss.at[0])
         gone(z_out.at[:len(early_groups) * (z_n - 1)], z_ss.at[0])
 
@@ -532,7 +536,7 @@
             pltpu.VMEM((st_n, dw, hw), BF16),
             pltpu.VMEM((st_n, dw, hw), BF16),
             pltpu.VMEM((dw, hw), F32),
-            sem(2), sem(2), sem(2 * blocks), sem(2 * blocks), sem(2), sem(2 * blocks * (z_n + 1)),
+            sem(2), sem(2), sem(1), sem(2 * blocks), sem(2), sem(2 * blocks * (z_n + 1)),
             sem(1), sem(1), sem(1), sem(1), sem(3 + blocks),
         ],
         compiler_params=pltpu.CompilerParams(

time: 57.1 us -> 56.5 us (0.989)
  no operation moved by 1% of the time
where the time goes in v4:
time: 56.5 us; the launch traced here: 56.3 us
  Pallas kernels  55.6 us (98%)
  between operations  0.64 us (1%)
    pallas_call x1, Pallas kernels, main_call(): pl.pallas_call(functools.partial(main_kernel, st_n, tp_n, reads, slots, p...  53.6 us
    pallas_call x1, Pallas kernels, spread(): pl.pallas_call(spread_kernel, out_shape=(jax.ShapeDtypeStruct((passes, PL...  2.09 us

profile of v4, /device:TPU:0, one launch (start us, length us, event | category | flops | bytes accessed | tf_op | source)
XLA Modules:
  0.0 56.3 jit_solution(1489437303492077991)
XLA Ops:
  0.6 53.6 %main.1 = (f32[512,256]{1,0:T(8,128)S(1)}, bf16[16,64,256]{2,1,0:T(8,128)(2,1)S(1)}, f32[512,256]{1,0:T(8,128)S(1)}, s32[16]{0:T(128)S(1)}) custom-call(s32[2,4]{1,0:T(2,128)} %bitcast.4, bf16[32,64,2048]{2,1,0:T(8,128)(2,1)} %bitcast.3, bf16[512,2048]{1,0:T(8,128)(2,1)} %normed_h.1, bf16[2048,256]{1,0:T(8,128)(2,1)} %w_q_h.1, bf16[2048,256]{1,0:T(8,128)(2,1)} %w_g_h.1, ...), custom_call_target="tpu_custom_call" | custom-call | tf_op jit(solution)/shard_map/main/pallas_call | solution.py:508
  54.2 2.1 %spread.1 = (f32[32,64,256]{2,1,0:T(8,128)}, f32[512,256]{1,0:T(8,128)}, f32[512,256]{1,0:T(8,128)}) custom-call(s32[16]{0:T(128)S(1)} %get-tuple-element.10.ids_h, bf16[16,64,256]{2,1,0:T(8,128)(2,1)S(1)} %get-tuple-element.11.returned, f32[512,256]{1,0:T(8,128)S(1)} %get-tuple-element.12.rows, f32[512,256]{1,0:T(8,128)S(1)} %get-tuple-element.13.gqw), custom_call_target="tpu_custom_call" | custom-call | tf_op jit(solution)/shard_map/spread/pallas_call | solution.py:587

commit v5 on v4

--- a/solution.py
+++ b/solution.py
@@ -438,9 +438,10 @@
     for s in range(st_n * slots):
         r_out[s] = part[req_of[s]]
     for d in range(1, st_n):
+        reader = st_peer(reach(d))
         remote(
-            r_out.at[rows_at(st_peer(d), slots)], r_in.at[rows_at(me_st, slots)],
-            r_ss.at[0], r_rs.at[0], (st_peer(d), me_tp),
+            r_out.at[rows_at(reader, slots)], r_in.at[rows_at(me_st, slots)],
+            r_ss.at[0], r_rs.at[0], (reader, me_tp),
         ).start()
     r_in[rows_at(me_st, slots)] = r_out[rows_at(me_st, slots)]
 

time: 56.5 us -> 56.5 us (level)
  no operation moved by 1% of the time
where the time goes in v5:
time: 56.5 us; the launch traced here: 56.3 us
  Pallas kernels  55.6 us (98%)
  between operations  0.64 us (1%)
    pallas_call x1, Pallas kernels, main_call(): pl.pallas_call(functools.partial(main_kernel, st_n, tp_n, reads, slots, p...  53.6 us
    pallas_call x1, Pallas kernels, spread(): pl.pallas_call(spread_kernel, out_shape=(jax.ShapeDtypeStruct((passes, PL...  2.08 us

profile of v5, /device:TPU:0, one launch (start us, length us, event | category | flops | bytes accessed | tf_op | source)
XLA Modules:
  0.0 56.3 jit_solution(11287360739604785823)
XLA Ops:
  0.6 53.6 %main.1 = (f32[512,256]{1,0:T(8,128)S(1)}, bf16[16,64,256]{2,1,0:T(8,128)(2,1)S(1)}, f32[512,256]{1,0:T(8,128)S(1)}, s32[16]{0:T(128)S(1)}) custom-call(s32[2,4]{1,0:T(2,128)} %bitcast.4, bf16[32,64,2048]{2,1,0:T(8,128)(2,1)} %bitcast.3, bf16[512,2048]{1,0:T(8,128)(2,1)} %normed_h.1, bf16[2048,256]{1,0:T(8,128)(2,1)} %w_q_h.1, bf16[2048,256]{1,0:T(8,128)(2,1)} %w_g_h.1, ...), custom_call_target="tpu_custom_call" | custom-call | tf_op jit(solution)/shard_map/main/pallas_call | solution.py:509
  54.2 2.1 %spread.1 = (f32[32,64,256]{2,1,0:T(8,128)}, f32[512,256]{1,0:T(8,128)}, f32[512,256]{1,0:T(8,128)}) custom-call(s32[16]{0:T(128)S(1)} %get-tuple-element.10.ids_h, bf16[16,64,256]{2,1,0:T(8,128)(2,1)S(1)} %get-tuple-element.11.returned, f32[512,256]{1,0:T(8,128)S(1)} %get-tuple-element.12.rows, f32[512,256]{1,0:T(8,128)S(1)} %get-tuple-element.13.gqw), custom_call_target="tpu_custom_call" | custom-call | tf_op jit(solution)/shard_map/spread/pallas_call | solution.py:588
